TPU v7x, 32 devices: a whole 2x2x4 slice. The times are simulated.
32 devices in a mesh: sp: 8 (over z, y), tp: 4 (over x, core).
Axes of the slice: x: 2, y: 2, z: 4, core: 2. Of those that a mesh axis runs over, the one named last changes fastest.
Arguments:
- glu_value: bfloat16 [8192, 1024], P('sp', 'tp'), may hold values from -6 to 6
- glu_gate: bfloat16 [8192, 1024], P('sp', 'tp'), may hold values from -8 to 8
- conv_taps: float32 [31, 1024], P(None, 'tp'), may hold values from -1 to 1
- channel_gain: float32 [1024], P('tp'), may hold values from 0.1 to 1.9
- proj_weight: bfloat16 [1024, 1024], P('tp'), may hold values from -0.1875 to 0.1875
- out_grad: bfloat16 [8192, 1024], P('sp'), may hold values from -6 to 6
Outputs:
- value_grad: bfloat16 [8192, 1024], P('sp', 'tp')
- gate_grad: bfloat16 [8192, 1024], P('sp', 'tp')
- proj_grad: float32 [1024, 1024], P(('tp', 'sp'))
- taps_grad: float32 [31, 1024], P(None, 'tp')
- norm_gain_gradient: float32 [1024], P('tp')
All inputs are finite; a program needn't handle non-finite values.
Results may differ from a plain program's by a relative error of at most 0.0029.
Values may be sent and summed in bfloat16 or wider, within the bound.
A program may use at most 64 MiB of HBM per device.

v0:
```python
import jax
import jax.numpy as jnp
from jax import lax
from jax.sharding import PartitionSpec as P


def from_behind(block, axis, distance):
    devices = range(lax.axis_size(axis))
    route = [(i - distance, i) for i in devices if i - distance in devices]
    return lax.ppermute(block, axis, route)


def per_device(glu_value, glu_gate, conv_taps, channel_gain, proj_weight, out_grad):
    kernel_len = conv_taps.shape[0]
    halo_rows = kernel_len - 1
    row_count = glu_value.shape[0]
    channel_width = channel_gain.shape[0] * lax.axis_size("tp")
    gradient_factor = 1.0 / jnp.sqrt(jnp.float32(row_count * lax.axis_size("sp")))
    prev_value, prev_gate = from_behind(
        (glu_value[row_count - halo_rows :], glu_gate[row_count - halo_rows :]), "sp", 1
    )
    next_value, next_gate, next_grad = from_behind(
        (glu_value[:halo_rows], glu_gate[:halo_rows], out_grad[:halo_rows]), "sp", -1
    )
    value_ext = jnp.concatenate([prev_value, glu_value, next_value], axis=0)
    gate_ext = jnp.concatenate([prev_gate, glu_gate, next_gate], axis=0)
    cot_ext = jnp.concatenate([out_grad, next_grad], axis=0)
    ext_count = row_count + halo_rows
    glu_out = value_ext.astype(jnp.float32) * jax.nn.sigmoid(gate_ext.astype(jnp.float32))
    convolved_output = jnp.zeros((ext_count, glu_out.shape[1]), jnp.float32)
    for tap in range(kernel_len):
        convolved_output = convolved_output + conv_taps[tap] * glu_out[tap : tap + ext_count]
    row_sum, row_sq = lax.psum(
        (jnp.sum(convolved_output, axis=1), jnp.sum(convolved_output * convolved_output, axis=1)),
        "tp",
    )
    row_average = (row_sum / channel_width)[:, None]
    inverse_deviation = lax.rsqrt(
        (row_sq / channel_width)[:, None] - row_average * row_average + 1e-05
    )
    centered_scaled = (convolved_output - row_average) * inverse_deviation
    normalized_rows = centered_scaled * channel_gain
    activ = jax.nn.silu(normalized_rows).astype(jnp.bfloat16)
    act_grad = lax.dot_general(
        cot_ext, proj_weight, (((1,), (1,)), ((), ())), preferred_element_type=jnp.float32
    )
    norm_sig = jax.nn.sigmoid(normalized_rows)
    normalized_gradient = act_grad * norm_sig * (1.0 + normalized_rows * (1.0 - norm_sig))
    centered_scaled_gradient = normalized_gradient * channel_gain
    backward_first, backward_second = lax.psum(
        (
            jnp.sum(centered_scaled_gradient, axis=1),
            jnp.sum(centered_scaled_gradient * centered_scaled, axis=1),
        ),
        "tp",
    )
    convolved_gradient = inverse_deviation * (
        centered_scaled_gradient
        - (backward_first / channel_width)[:, None]
        - centered_scaled * (backward_second / channel_width)[:, None]
    )
    own_grad = convolved_gradient[:row_count]
    gain_product = (
        jnp.sum(normalized_gradient[:row_count] * centered_scaled[:row_count], axis=0)
        * gradient_factor
    )
    taps_term = (
        jnp.stack(
            [
                jnp.sum(own_grad * glu_out[tap : tap + row_count], axis=0)
                for tap in range(kernel_len)
            ]
        )
        * gradient_factor
    )
    glu_grad = jnp.zeros((row_count, glu_out.shape[1]), jnp.float32)
    for tap in range(kernel_len):
        glu_grad = (
            glu_grad
            + conv_taps[tap] * convolved_gradient[halo_rows - tap : halo_rows - tap + row_count]
        )
    value_f = glu_value.astype(jnp.float32)
    gate_sig = jax.nn.sigmoid(glu_gate.astype(jnp.float32))
    value_grad = (glu_grad * gate_sig).astype(jnp.bfloat16)
    gate_grad = (glu_grad * value_f * gate_sig * (1.0 - gate_sig)).astype(jnp.bfloat16)
    own_activ = activ[:row_count]
    proj_grad = lax.psum_scatter(
        lax.dot_general(
            own_activ, out_grad, (((0,), (0,)), ((), ())), preferred_element_type=jnp.float32
        )
        * gradient_factor,
        "sp",
        scatter_dimension=0,
        tiled=True,
    )
    taps_grad, norm_gain_gradient = lax.psum((taps_term, gain_product), "sp")
    return (value_grad, gate_grad, proj_grad, taps_grad, norm_gain_gradient)


def solution(mesh):
    return jax.shard_map(
        per_device,
        mesh=mesh,
        in_specs=(
            P("sp", "tp"),
            P("sp", "tp"),
            P(None, "tp"),
            P("tp"),
            P("tp", None),
            P("sp", None),
        ),
        out_specs=(P("sp", "tp"), P("sp", "tp"), P(("tp", "sp"), None), P(None, "tp"), P("tp")),
        check_vma=False,
    )
```

profile of v0, /device:TPU:0, one launch (start us, length us, event | category | flops | bytes accessed | tf_op | source)
XLA Modules:
  0.0 126.2 jit_solution(16626724161124096512)
XLA Ops:
  7.2 0.0 copy-start
  7.2 0.0 copy-start.5
  7.2 0.0 reduce-scatter.2.cloned.1.call-start
  7.2 0.8 fusion.101
  8.1 1.3 %collective-permute-start.1 = (bf16[30,256]{1,0:T(8,128)(2,1)S(1)}, bf16[30,256]{1,0:T(8,128)(2,1)S(1)}, u32[]{:S(2)}, u32[]{:S(2)}) collective-permute-start(bf16[30,256]{1,0:T(8,128)(2,1)S(1)} %get-tuple-element.56), channel_id=1, source_target_pairs={{4,0},{8,4},{12,8},{16,12},{20,16},{24,20},{28,24},{5,1},{9,5},{13... | collective-permute-start | bytes 46088 | tf_op jit(solution)/shard_map/ppermute | solution.py:10
  9.4 5.5 %collective-permute-start = (bf16[30,256]{1,0:T(8,128)(2,1)S(1)}, bf16[30,256]{1,0:T(8,128)(2,1)S(1)}, u32[]{:S(2)}, u32[]{:S(2)}) collective-permute-start(bf16[30,256]{1,0:T(8,128)(2,1)S(1)} %get-tuple-element.57), channel_id=1, source_target_pairs={{0,4},{4,8},{8,12},{12,16},{16,20},{20,24},{24,28},{1,5},{5,9},{9,... | collective-permute-start | bytes 46088 | tf_op jit(solution)/shard_map/ppermute | solution.py:10
  14.9 0.7 fusion.102
  15.6 1.3 %collective-permute-start.3 = (bf16[30,256]{1,0:T(8,128)(2,1)S(1)}, bf16[30,256]{1,0:T(8,128)(2,1)S(1)}, u32[]{:S(2)}, u32[]{:S(2)}) collective-permute-start(bf16[30,256]{1,0:T(8,128)(2,1)S(1)} %get-tuple-element.58), channel_id=1, source_target_pairs={{4,0},{8,4},{12,8},{16,12},{20,16},{24,20},{28,24},{5,1},{9,5},{13... | collective-permute-start | bytes 46088 | tf_op jit(solution)/shard_map/ppermute | solution.py:10
  16.9 5.4 %collective-permute-start.2 = (bf16[30,256]{1,0:T(8,128)(2,1)S(1)}, bf16[30,256]{1,0:T(8,128)(2,1)S(1)}, u32[]{:S(2)}, u32[]{:S(2)}) collective-permute-start(bf16[30,256]{1,0:T(8,128)(2,1)S(1)} %get-tuple-element.59), channel_id=1, source_target_pairs={{0,4},{4,8},{8,12},{12,16},{16,20},{20,24},{24,28},{1,5},{5,9},{9,... | collective-permute-start | bytes 46088 | tf_op jit(solution)/shard_map/ppermute | solution.py:10
  22.4 0.8 slice.494
  23.2 1.3 %collective-permute-start.4 = (bf16[30,1024]{1,0:T(8,128)(2,1)S(1)}, bf16[30,1024]{1,0:T(8,128)(2,1)S(1)}, u32[]{:S(2)}, u32[]{:S(2)}) collective-permute-start(bf16[30,1024]{1,0:T(8,128)(2,1)S(1)} %slice.494), channel_id=1, source_target_pairs={{4,0},{8,4},{12,8},{16,12},{20,16},{24,20},{28,24},{5,1},{9,5},{13... | collective-permute-start | bytes 184328 | tf_op jit(solution)/shard_map/ppermute | solution.py:10
  24.5 1.0 fusion.103
  25.5 1.0 fusion.104
  26.5 0.0 collective-permute-done.3
  26.5 0.0 collective-permute-done.2
  26.5 3.1 %concatenate.10 = bf16[1084,256]{1,0:T(8,128)(2,1)S(1)} concatenate(bf16[30,256]{1,0:T(8,128)(2,1)S(1)} %collective-permute-done.2, bf16[1024,256]{1,0:T(8,128)(2,1)} %param.7, bf16[30,256]{1,0:T(8,128)(2,1)S(1)} %collective-permute-done.3), dimensions={0} | concatenate | bytes 1110016 | tf_op jit(solution)/shard_map/concatenate | solution.py:26
  29.7 0.0 collective-permute-done.1
  29.7 0.0 collective-permute-done
  29.7 0.0 copy-done.5
  29.7 1.0 concatenate.9
  30.7 0.3 divide_multiply_fusion
  31.0 0.0 copy-start.7
  31.0 5.4 %multiply_reduce_fusion.1 = (f32[1054]{0:T(1024)S(1)}, f32[1054]{0:T(1024)S(1)}, f32[1054,256]{1,0:T(8,128)}) fusion(f32[1084,256]{1,0:T(8,128)S(1)} %divide_multiply_fusion, f32[256]{0:T(256)S(1)} %bitcast.122, f32[256]{0:T(256)S(1)} %bitcast.124, f32[256]{0:T(256)S(1)} %bitcast.66, f32[256]{0:T(256)S(1)} %bitcast.68, f32[256]{0:T(256)S(1)} %bitcast.70, ...), kind=kLoop, calls=%fused_computation.72 | loop fusion | flops 17266628 | bytes 34577648 | tf_op jit(solution)/shard_map/reduce_sum | solution.py:34
  36.4 10.1 %all-reduce.2 = (f32[1054]{0:T(1024)S(1)}, f32[1054]{0:T(1024)S(1)}) all-reduce(f32[1054]{0:T(1024)S(1)} %get-tuple-element.39, f32[1054]{0:T(1024)S(1)} %get-tuple-element.38), channel_id=1, replica_groups=mesh['sp'=8,'tp'=4] {'tp'}, use_global_device_ids=true, to_apply=%region_3.0 | all-reduce | flops 2108 | bytes 16864 | tf_op jit(solution)/shard_map/psum | solution.py:33
  46.5 0.0 copy-done.7
  46.5 0.0 copy-start.6
  46.6 1.8 %add_divide_fusion = (f32[1054,256]{1,0:T(8,128)S(1)}, f32[1054,256]{1,0:T(8,128)S(1)}, f32[1054,256]{1,0:T(8,128)S(1)}) fusion(f32[256]{0:T(256)S(1)} %copy-done.7, f32[1054]{0:T(1024)S(1)} %get-tuple-element.92, f32[1054,256]{1,0:T(8,128)} %get-tuple-element.51, f32[1054]{0:T(1024)S(1)} %get-tuple-element.91), kind=kLoop, calls=%fused_computation.70 | loop fusion | flops 1618944 | bytes 4326640 | tf_op jit(solution)/shard_map/div | solution.py:47
  48.3 0.0 copy-start.3
  48.3 0.0 copy-start.1
  48.3 1.0 copy-done.3
  49.4 0.0 copy-done.6
  49.4 1.7 %convolution_multiply_fusion.1 = f32[256,1024]{1,0:T(8,128)} fusion(bf16[1024,1024]{1,0:T(8,128)(2,1)S(1)} %copy-done.6, f32[1054,256]{1,0:T(8,128)S(1)} %get-tuple-element.46, f32[1054,256]{1,0:T(8,128)S(1)} %get-tuple-element.47), kind=kOutput, calls=%fused_computation.5 | convolution fusion | flops 537657344 | bytes 5242880 | tf_op jit(solution)/shard_map/dot_general | solution.py:88
  51.1 0.0 reduce-scatter.2.cloned.1.call-update
  51.1 0.0 collective-permute-done.4
  51.1 3.0 %multiply_reduce_fusion.2 = (f32[1054]{0:T(1024)S(1)}, f32[1054]{0:T(1024)S(1)}, f32[1054,256]{1,0:T(8,128)S(1)}) fusion(f32[256]{0:T(256)S(1)} %copy-done.7, f32[1054,256]{1,0:T(8,128)S(1)} %get-tuple-element.48, f32[1054,256]{1,0:T(8,128)} %copy-done.3, bf16[256,1024]{1,0:T(8,128)(2,1)S(1)} %copy-done, bf16[30,1024]{1,0:T(8,128)(2,1)S(1)} %collective-permute-done.4, ...), kind=kOutput, calls=%fused_computation.202 | convolution fusion | flops 560152576 | bytes 5930224 | tf_op jit(solution)/shard_map/dot_general | solution.py:44
  54.1 0.3 fusion.34
  54.4 0.7 copy-done.4
  55.2 10.1 %all-reduce.1 = (f32[1054]{0:T(1024)S(1)}, f32[1054]{0:T(1024)S(1)}) all-reduce(f32[1054]{0:T(1024)S(1)} %get-tuple-element.37, f32[1054]{0:T(1024)S(1)} %get-tuple-element.36), channel_id=1, replica_groups=mesh['sp'=8,'tp'=4] {'tp'}, use_global_device_ids=true, to_apply=%region_7.8 | all-reduce | flops 2108 | bytes 16864 | tf_op jit(solution)/shard_map/psum | solution.py:50
  65.3 2.0 %subtract_multiply_fusion = f32[1054,256]{1,0:T(8,128)S(1)} fusion(f32[1054,256]{1,0:T(8,128)} %copy-done.1, f32[1054,256]{1,0:T(8,128)} %copy-done.4, f32[1054]{0:T(1024)S(1)} %get-tuple-element.94, f32[1054]{0:T(1024)S(1)} %get-tuple-element.95, f32[256]{0:T(256)S(1)} %copy-done.7, f32[1054]{0:T(1024)S(1)} %get-tuple-element.92), kind=kLoop, calls=%fused_computation.68 | loop fusion | flops 1349120 | bytes 3251560 | tf_op jit(solution)/shard_map/mul | solution.py:57
  67.3 1.1 fusion.35
  68.5 1.1 fusion.52
  69.6 0.0 copy-start.2
  69.6 1.8 %fusion.43 = (f32[256]{0:T(256)S(1)}, f32[256]{0:T(256)S(1)}, f32[256]{0:T(256)S(1)}, f32[256]{0:T(256)S(1)}, f32[256]{0:T(256)S(1)}, /*index=5*/f32[256]{0:T(25...) fusion(f32[1084,256]{1,0:T(8,128)S(1)} %divide_multiply_fusion,, ...), kind=kLoop, calls=%fused_computation.92 | loop fusion | flops 6812416 | bytes 14693376 | tf_op jit(solution)/shard_map/reduce_sum | solution.py:70
  71.4 0.1 stack.127
  71.5 39.9 %all-reduce = (f32[31,256]{1,0:T(8,128)}, f32[256]{0:T(256)}) all-reduce(f32[31,256]{1,0:T(8,128)S(1)} %broadcast_multiply_fusion.1, f32[256]{0:T(256)S(1)} %broadcast_multiply_fusion.5), channel_id=1, replica_groups=mesh['sp'=8,'tp'=4] {'sp'}, use_global_device_ids=true, to_apply=%region_40.41 | all-reduce | flops 8192 | bytes 65536 | tf_op jit(solution)/shard_map/psum | solution.py:96
  111.4 6.0 %multiply_convert_fusion = (bf16[1024,256]{1,0:T(8,128)(2,1)}, f32[1024,256]{1,0:T(8,128)S(1)}) fusion(bf16[1024,256]{1,0:T(8,128)(2,1)} %param.6, bf16[1024,256]{1,0:T(8,128)(2,1)S(1)} %copy-done.2, f32[1054,256]{1,0:T(8,128)S(1)} %subtract_multiply_fusion, f32[256]{0:T(256)S(1)} %bitcast.123, f32[256]{0:T(256)S(1)} %bitcast.125, f32[256]{0:T(256)S(1)} %bitcast.67, ...), kind=kLoop, calls=%fused_computation.199 | loop fusion | flops 18612224 | bytes 35159040 | tf_op jit(solution)/shard_map/convert_element_type | solution.py:85
  117.4 1.1 multiply_convert_fusion.1
  118.5 0.8 reduce-scatter.2.cloned.1.call-done
  (8 shorter events, 0.0 us)
Async XLA Ops:
  7.2 44.0 %copy-start = (bf16[256,1024]{1,0:T(8,128)(2,1)S(1)}, bf16[256,1024]{1,0:T(8,128)(2,1)}, u32[]{:S(2)}) copy-start(bf16[256,1024]{1,0:T(8,128)(2,1)} %param.10) | copy-start | bytes 1572868
  7.2 22.5 %copy-start.5 = (bf16[1024,256]{1,0:T(8,128)(2,1)S(1)}, bf16[1024,256]{1,0:T(8,128)(2,1)}, u32[]{:S(2)}) copy-start(bf16[1024,256]{1,0:T(8,128)(2,1)} %param.6) | copy-start | bytes 1572868
  7.2 112.1 %reduce-scatter.2.cloned.1.call-start = ((), (), s32[]{:S(2)}) async-start(), calls=%async_computation.1 | async-start | bytes 1179648 | tf_op jit(solution)/shard_map/reduce_scatter | solution.py:87
  8.1 21.6 %collective-permute-start.1 = (bf16[30,256]{1,0:T(8,128)(2,1)S(1)}, bf16[30,256]{1,0:T(8,128)(2,1)S(1)}, u32[]{:S(2)}, u32[]{:S(2)}) collective-permute-start(bf16[30,256]{1,0:T(8,128)(2,1)S(1)} %get-tuple-element.56), channel_id=1, source_target_pairs={{4,0},{8,4},{12,8},{16,12},{20,16},{24,20},{28,24},{5,1},{9,5},{13... | collective-permute-start | bytes 46088 | tf_op jit(solution)/shard_map/ppermute | solution.py:10
  9.4 20.3 %collective-permute-start = (bf16[30,256]{1,0:T(8,128)(2,1)S(1)}, bf16[30,256]{1,0:T(8,128)(2,1)S(1)}, u32[]{:S(2)}, u32[]{:S(2)}) collective-permute-start(bf16[30,256]{1,0:T(8,128)(2,1)S(1)} %get-tuple-element.57), channel_id=1, source_target_pairs={{0,4},{4,8},{8,12},{12,16},{16,20},{20,24},{24,28},{1,5},{5,9},{9,... | collective-permute-start | bytes 46088 | tf_op jit(solution)/shard_map/ppermute | solution.py:10
  15.6 10.9 %collective-permute-start.3 = (bf16[30,256]{1,0:T(8,128)(2,1)S(1)}, bf16[30,256]{1,0:T(8,128)(2,1)S(1)}, u32[]{:S(2)}, u32[]{:S(2)}) collective-permute-start(bf16[30,256]{1,0:T(8,128)(2,1)S(1)} %get-tuple-element.58), channel_id=1, source_target_pairs={{4,0},{8,4},{12,8},{16,12},{20,16},{24,20},{28,24},{5,1},{9,5},{13... | collective-permute-start | bytes 46088 | tf_op jit(solution)/shard_map/ppermute | solution.py:10
  16.9 9.6 %collective-permute-start.2 = (bf16[30,256]{1,0:T(8,128)(2,1)S(1)}, bf16[30,256]{1,0:T(8,128)(2,1)S(1)}, u32[]{:S(2)}, u32[]{:S(2)}) collective-permute-start(bf16[30,256]{1,0:T(8,128)(2,1)S(1)} %get-tuple-element.59), channel_id=1, source_target_pairs={{0,4},{4,8},{8,12},{12,16},{16,20},{20,24},{24,28},{1,5},{5,9},{9,... | collective-permute-start | bytes 46088 | tf_op jit(solution)/shard_map/ppermute | solution.py:10
  23.2 27.9 %collective-permute-start.4 = (bf16[30,1024]{1,0:T(8,128)(2,1)S(1)}, bf16[30,1024]{1,0:T(8,128)(2,1)S(1)}, u32[]{:S(2)}, u32[]{:S(2)}) collective-permute-start(bf16[30,1024]{1,0:T(8,128)(2,1)S(1)} %slice.494), channel_id=1, source_target_pairs={{4,0},{8,4},{12,8},{16,12},{20,16},{24,20},{28,24},{5,1},{9,5},{13... | collective-permute-start | bytes 184328 | tf_op jit(solution)/shard_map/ppermute | solution.py:10
  31.0 15.6 %copy-start.7 = (f32[256]{0:T(256)S(1)}, f32[256]{0:T(256)}, u32[]{:S(2)}) copy-start(f32[256]{0:T(256)} %param.9) | copy-start | bytes 3076
  46.5 2.8 %copy-start.6 = (bf16[1024,1024]{1,0:T(8,128)(2,1)S(1)}, bf16[1024,1024]{1,0:T(8,128)(2,1)}, u32[]{:S(2)}) copy-start(bf16[1024,1024]{1,0:T(8,128)(2,1)} %param.11) | copy-start | bytes 6291460
  48.3 1.0 copy-start.3
  48.3 5.8 %copy-start.1 = (f32[1054,256]{1,0:T(8,128)}, f32[1054,256]{1,0:T(8,128)S(1)}, u32[]{:S(2)}) copy-start(f32[1054,256]{1,0:T(8,128)S(1)} %get-tuple-element.48) | copy-start | bytes 3237892
  54.1 1.0 copy-start.4
  69.6 41.8 %copy-start.2 = (bf16[1024,256]{1,0:T(8,128)(2,1)S(1)}, bf16[1024,256]{1,0:T(8,128)(2,1)}, u32[]{:S(2)}) copy-start(bf16[1024,256]{1,0:T(8,128)(2,1)} %param.7) | copy-start | bytes 1572868
Sparse Core Ops, SparseCore 0:
  51.2 68.0 reduce-scatter.1
where the time goes:
time: 127 us; the launch traced here: 126 us
  blocking collectives  60.2 us (47%)
  other arithmetic  20.9 us (16%)
  starting transfers between devices  14.9 us (12%)
  between operations  14.3 us (11%)
  local copies, waits for them, and re-layouts  10.4 us (8%)
  matrix products  4.72 us (4%)
    psum x1, blocking collectives, per_device(): taps_grad, norm_gain_gradient = lax.psum((taps_term, gain_product), 'sp')  39.9 us
    ppermute x5, starting transfers between devices, from_behind(): return lax.ppermute(block, axis, route)  14.8 us
    psum x1, blocking collectives, per_device(): lax.psum((jnp.sum(convolved_output, axis=1), jnp.sum(convolved_output * c...  10.1 us
    psum x1, blocking collectives, per_device(): lax.psum((jnp.sum(centered_scaled_gradient, axis=1), jnp.sum(centered_sca...  10.1 us
    convert_element_type x1, other arithmetic, per_device(): (glu_grad * value_f * gate_sig * (1.0 - gate_sig)).astype(jnp.bfloat16)  6.04 us
    reduce_sum x1, other arithmetic, per_device(): jnp.sum(convolved_output * convolved_output, axis=1)  5.4 us
    reduce_sum x3, other arithmetic, per_device(): jnp.sum(own_grad * glu_out[tap:tap + row_count], axis=0)  3.98 us
    concatenate x1, local copies, waits for them, and re-layouts, per_device(): gate_ext = jnp.concatenate([prev_gate, glu_gate, next_gate], axis=0)  3.1 us
  transfers between devices with their start and end apart: 6, of which 1 were waited for; matrix products, arithmetic and copies ran while one was open for 26% of the time, Pallas kernels for 0%

commit v1 on v0

v1 whole, which is shorter than its diff:
```python
import functools

import jax
import jax.numpy as jnp
from jax import lax
from jax.experimental import pallas as pl
from jax.experimental.pallas import tpu as pltpu

MESH = pl.DeviceIdType.MESH
F32 = jnp.float32
BF16 = jnp.bfloat16
LANES = 128
BLOCK = 128


def split_two(x):
    hi = x.astype(BF16)
    return hi, (x - hi.astype(F32)).astype(BF16)


def split_three(x):
    hi = x.astype(BF16).astype(F32)
    rest = x - hi
    mid = rest.astype(BF16).astype(F32)
    low = (rest - mid).astype(BF16).astype(F32)
    return [hi, mid, low]


def nt(a, b):
    return lax.dot_general(a, b, (((1,), (1,)), ((), ())), preferred_element_type=F32)


def nn(a, b):
    return lax.dot_general(a, b, (((1,), (0,)), ((), ())), preferred_element_type=F32)


def kernel(
    cfg,
    value_hbm, gate_hbm, taps_ref, gain_ref, weight_hbm, cot_hbm,
    vgrad_hbm, ggrad_hbm, proj_out, taps_out,
    value_v, gate_v, weight_v, cot_v, halo_v, halo_g, gsig, glu, xbuf, cg, act_t,
    taps_b, taps_acc, st1, st1_in, st2, st2_in, rs_send, rs_own, rs_in,
    tg_send, tg_in, vout, gout,
    in_sem, out_sem, halo_send, halo_recv, cgs_send, cgs_recv,
    s1_send, s1_recv, s2_send, s2_recv, rs_ssem, rs_rsem, tg_ssem, tg_rsem,
):
    rows, width, klen, halo, n_sp, n_tp, fused = cfg
    halves = width // LANES
    blocks = rows // BLOCK
    channels = width * n_tp
    lead = halo - (klen - 1)
    factor = 1.0 / jnp.sqrt(F32(rows * n_sp))
    sp = lax.axis_index("sp")
    tp = lax.axis_index("tp")

    loads = [
        pltpu.make_async_copy(src, dst, in_sem.at[i])
        for i, (src, dst) in enumerate(
            [(value_hbm, value_v), (gate_hbm, gate_v), (weight_hbm, weight_v), (cot_hbm, cot_v)]
        )
    ]
    for copy in loads:
        copy.start()

    barrier = pltpu.get_barrier_semaphore()
    sp_hops = list(range(1, n_sp)) if fused else [1, n_sp - 1]
    for o in sp_hops:
        pl.semaphore_signal(
            barrier, inc=1, device_id=(lax.rem(sp + o, n_sp), tp), device_id_type=MESH
        )
    for o in range(1, n_tp):
        pl.semaphore_signal(
            barrier, inc=1, device_id=(sp, lax.rem(tp + o, n_tp)), device_id_type=MESH
        )

    for k in range(klen):
        taps_b[k] = jnp.broadcast_to(taps_ref[k : k + 1, :], (8, width))
    taps_acc[...] = jnp.zeros_like(taps_acc)
    st1[...] = jnp.zeros_like(st1)
    st2[...] = jnp.zeros_like(st2)

    loads[0].wait()
    loads[1].wait()
    pl.semaphore_wait(barrier, len(sp_hops) + n_tp - 1)

    nxt = (jnp.minimum(sp + 1, n_sp - 1), tp)
    prv = (jnp.maximum(sp - 1, 0), tp)

    def halo_copies():
        tail = pl.ds(rows - halo, halo)
        return [
            pltpu.make_async_remote_copy(
                src_ref=src.at[tail], dst_ref=dst, send_sem=halo_send.at[i],
                recv_sem=halo_recv.at[i], device_id=nxt, device_id_type=MESH,
            )
            for i, (src, dst) in enumerate([(value_v, halo_v), (gate_v, halo_g)])
        ]

    @pl.when(sp < n_sp - 1)
    def _():
        for copy in halo_copies():
            copy.start()

    def rows_of(c):
        return pl.ds(pl.multiple_of(c * BLOCK, BLOCK), BLOCK)

    def glu_block(c, carry):
        at = rows_of(c)
        to = pl.ds(pl.multiple_of(c * BLOCK + halo, 8), BLOCK)
        sig = jax.nn.sigmoid(gate_v[at, :].astype(F32))
        out = value_v[at, :].astype(F32) * sig
        for h in range(halves):
            cols = slice(h * LANES, (h + 1) * LANES)
            gsig[h, at, :] = sig[:, cols]
            glu[h, to, :] = out[:, cols]
        return carry

    lax.fori_loop(0, blocks, glu_block, 0)

    def conv_block(src, h, base, first, tap_of):
        cols = slice(h * LANES, (h + 1) * LANES)
        acc = None
        for s in range(8):
            qs = [q for q in range((first + klen + 7) // 8 + 1) if first <= 8 * q + s < first + klen]
            if not qs:
                continue
            lo = qs[0]
            span = BLOCK + 8 * (qs[-1] - lo)
            slab = src[h, pl.ds(base + (8 * lo + s), span), :]
            for q in qs:
                tap = taps_b[tap_of(8 * q + s - first), :, cols]
                part = slab[8 * (q - lo) : 8 * (q - lo) + BLOCK]
                term = part.reshape(BLOCK // 8, 8, LANES) * tap[None]
                acc = term if acc is None else acc + term
        return acc.reshape(BLOCK, LANES)

    def place_sums(ref, c, first, second):
        which = lax.broadcasted_iota(jnp.int32, (16, width), 0)
        one = jnp.where(which == c, 1.0, 0.0).astype(BF16)
        two = jnp.where(which == c + 8, 1.0, 0.0).astype(BF16)
        total = ref[...]
        for sel, x in ((one, first), (two, second)):
            hi, low = split_two(x)
            total = total + nt(sel, hi) + nt(sel, low)
        ref[...] = total

    def forward_block(c):
        base = c * BLOCK
        at = rows_of(c)
        parts = []
        for h in range(halves):
            out = conv_block(glu, h, base, lead, lambda k: k)
            xbuf[h, at, :] = out
            parts.append(out)
        x = jnp.concatenate(parts, axis=1)
        place_sums(st1, c, x, x * x)

    def fwd_loop(c, carry):
        forward_block(c)
        return carry

    lax.fori_loop(1, blocks, fwd_loop, 0)

    @pl.when(sp > 0)
    def _():
        for copy in halo_copies():
            copy.wait_recv()
        out = halo_v[...].astype(F32) * jax.nn.sigmoid(halo_g[...].astype(F32))
        for h in range(halves):
            glu[h, 0:halo, :] = out[:, h * LANES : (h + 1) * LANES]

    @pl.when(sp == 0)
    def _():
        for h in range(halves):
            glu[h, 0:halo, :] = jnp.zeros((halo, LANES), F32)

    lax.fori_loop(0, 1, fwd_loop, 0)

    def tp_copies(src, dst, ssem, rsem):
        return [
            pltpu.make_async_remote_copy(
                src_ref=src, dst_ref=dst.at[o - 1], send_sem=ssem.at[o - 1],
                recv_sem=rsem.at[o - 1], device_id=(sp, lax.rem(tp + o, n_tp)),
                device_id_type=MESH,
            )
            for o in range(1, n_tp)
        ]

    ex1 = tp_copies(st1, st1_in, s1_send, s1_recv)
    for copy in ex1:
        copy.start()
    loads[2].wait()
    loads[3].wait()

    def act_grad_block(c, carry):
        at = rows_of(c)
        out = nt(cot_v[at, :], weight_v[...])
        for h in range(halves):
            cg[h, at, :] = out[:, h * LANES : (h + 1) * LANES]
        return carry

    lax.fori_loop(0, blocks, act_grad_block, 0)
    for copy in ex1:
        copy.wait_recv()

    total = st1[...]
    for o in range(n_tp - 1):
        total = total + st1_in[o]
    mean = total[0:8] / channels
    rstd = lax.rsqrt(total[8:16] / channels - mean * mean + 1e-05)

    def columns(a, b):
        stack = split_three(a) + split_three(b)
        stack.append(jnp.zeros((LANES - 48, LANES), F32))
        return jnp.transpose(jnp.concatenate(stack, axis=0)).astype(BF16)

    def spread(cols, c):
        k = lax.broadcasted_iota(jnp.int32, (LANES, 2 * LANES), 0)
        j = lax.broadcasted_iota(jnp.int32, (LANES, 2 * LANES), 1)
        low = jnp.where(j < LANES, 0, 24)
        hit = (k == c + low) | (k == c + low + 8) | (k == c + low + 16)
        out = nn(cols, jnp.where(hit, 1.0, 0.0).astype(BF16))
        return out[:, :LANES], out[:, LANES:]

    cols1 = columns(mean, rstd)

    def norm_block(c, carry):
        at = rows_of(c)
        mean_b, rstd_b = spread(cols1, c)
        firsts, seconds, activs = [], [], []
        for h in range(halves):
            cols = slice(h * LANES, (h + 1) * LANES)
            gain = gain_ref[0:1, cols]
            xhat = (xbuf[h, at, :] - mean_b) * rstd_b
            normed = xhat * gain
            sig = jax.nn.sigmoid(normed)
            activs.append(normed * sig)
            ngrad = cg[h, at, :] * sig * (1.0 + normed * (1.0 - sig))
            xgrad = ngrad * gain
            taps_acc[klen, :, cols] += jnp.sum(
                (ngrad * xhat).reshape(BLOCK // 8, 8, LANES), axis=0
            )
            xbuf[h, at, :] = xhat
            cg[h, at, :] = xgrad
            firsts.append(xgrad)
            seconds.append(xgrad * xhat)
        place_sums(st2, c, jnp.concatenate(firsts, axis=1), jnp.concatenate(seconds, axis=1))
        activ = jnp.concatenate(activs, axis=1)
        act_t[:, at] = jnp.transpose(activ).astype(BF16)
        return carry

    lax.fori_loop(0, blocks, norm_block, 0)

    ex2 = tp_copies(st2, st2_in, s2_send, s2_recv)
    for copy in ex2:
        copy.start()

    out_cols = proj_out.shape[-1]
    tile = 256
    hops = list(range(1, n_sp)) if fused else []
    hops.sort(key=lambda o: -min(o, n_sp - o))

    def rs_copy(o, cols):
        dest = lax.rem(sp + o, n_sp)
        return pltpu.make_async_remote_copy(
            src_ref=rs_send.at[dest, :, cols], dst_ref=rs_in.at[o - 1, :, cols],
            send_sem=rs_ssem.at[o - 1], recv_sem=rs_rsem.at[o - 1],
            device_id=(dest, tp), device_id_type=MESH,
        )

    for nb in range(out_cols // tile):
        cols = slice(nb * tile, (nb + 1) * tile)
        part = nn(act_t[...], cot_v[:, cols]) * factor
        if fused:
            own = width // n_sp
            rs_own[:, :, cols] = part.reshape(n_sp, own, tile)
            rs_send[:, :, cols] = part.astype(BF16).reshape(n_sp, own, tile)
            for o in hops:
                rs_copy(o, pl.ds(nb * tile, tile)).start()
        else:
            proj_out[:, cols] = part

    for copy in ex2:
        copy.wait_recv()
    total = st2[...]
    for o in range(n_tp - 1):
        total = total + st2_in[o]
    cols2 = columns(total[0:8] / channels, total[8:16] / channels)

    def cgrad_block(c):
        at = rows_of(c)
        base = c * BLOCK
        _, rstd_b = spread(cols1, c)
        one_b, two_b = spread(cols2, c)
        for h in range(halves):
            cols = slice(h * LANES, (h + 1) * LANES)
            grad = rstd_b * (cg[h, at, :] - one_b - xbuf[h, at, :] * two_b)
            cg[h, at, :] = grad
            grad3 = grad.reshape(BLOCK // 8, 8, LANES)
            for s in range(8):
                qs = [q for q in range((lead + klen + 7) // 8 + 1) if lead <= 8 * q + s < lead + klen]
                if not qs:
                    continue
                lo = qs[0]
                span = BLOCK + 8 * (qs[-1] - lo)
                slab = glu[h, pl.ds(base + (8 * lo + s), span), :]
                for q in qs:
                    part = slab[8 * (q - lo) : 8 * (q - lo) + BLOCK]
                    prod = grad3 * part.reshape(BLOCK // 8, 8, LANES)
                    taps_acc[8 * q + s - lead, :, cols] += jnp.sum(prod, axis=0)

    def cgrad_loop(c, carry):
        cgrad_block(c)
        return carry

    lax.fori_loop(0, 1, cgrad_loop, 0)

    cg_copy = pltpu.make_async_remote_copy(
        src_ref=cg.at[:, pl.ds(0, halo), :], dst_ref=cg.at[:, pl.ds(rows, halo), :],
        send_sem=cgs_send, recv_sem=cgs_recv, device_id=prv, device_id_type=MESH,
    )

    @pl.when(sp > 0)
    def _():
        cg_copy.start()

    lax.fori_loop(1, blocks, cgrad_loop, 0)

    taps_sum = jnp.sum(taps_acc[...], axis=1) * factor
    taps_out[...] = taps_sum

    def tg_copy(o):
        return pltpu.make_async_remote_copy(
            src_ref=tg_send, dst_ref=tg_in.at[o - 1],
            send_sem=tg_ssem.at[o - 1], recv_sem=tg_rsem.at[o - 1],
            device_id=(lax.rem(sp + o, n_sp), tp), device_id_type=MESH,
        )

    if fused:
        tg_send[...] = taps_sum.astype(BF16)
        for o in hops:
            tg_copy(o).start()

    def out_copies(c):
        at = rows_of(c)
        return [
            pltpu.make_async_copy(vout.at[at], vgrad_hbm.at[at], out_sem.at[0, c]),
            pltpu.make_async_copy(gout.at[at], ggrad_hbm.at[at], out_sem.at[1, c]),
        ]

    def grad_loop(c, carry):
        at = rows_of(c)
        base = c * BLOCK
        for h in range(halves):
            cols = slice(h * LANES, (h + 1) * LANES)
            grad = conv_block(cg, h, base, 0, lambda j: klen - 1 - j)
            sig = gsig[h, at, :]
            scaled = grad * sig
            vout[at, cols] = scaled.astype(BF16)
            gout[at, cols] = (scaled * value_v[at, cols].astype(F32) * (1.0 - sig)).astype(BF16)
        for copy in out_copies(c):
            copy.start()
        return carry

    lax.fori_loop(0, blocks - 1, grad_loop, 0)

    @pl.when(sp < n_sp - 1)
    def _():
        cg_copy.wait_recv()

    @pl.when(sp == n_sp - 1)
    def _():
        for h in range(halves):
            cg[h, pl.ds(rows, halo), :] = jnp.zeros((halo, LANES), F32)

    lax.fori_loop(blocks - 1, blocks, grad_loop, 0)

    if fused:
        taps_total = taps_sum
        for o in range(1, n_sp):
            tg_copy(o).wait_recv()
            taps_total = taps_total + tg_in[o - 1].astype(F32)
        taps_out[...] = taps_total
        for o in hops:
            rs_copy(o, pl.ds(0, out_cols)).wait_recv()
        proj = rs_own[sp]
        for o in hops:
            proj = proj + rs_in[o - 1].astype(F32)
        proj_out[...] = proj
        for o in hops:
            rs_copy(o, pl.ds(0, out_cols)).wait_send()
            tg_copy(o).wait_send()
    for copy in ex1 + ex2:
        copy.wait_send()

    @pl.when(sp < n_sp - 1)
    def _():
        for copy in halo_copies():
            copy.wait_send()

    @pl.when(sp > 0)
    def _():
        cg_copy.wait_send()

    def drain(c, carry):
        for copy in out_copies(c):
            copy.wait()
        return carry

    lax.fori_loop(0, blocks, drain, 0)


def per_device(glu_value, glu_gate, conv_taps, channel_gain, proj_weight, out_grad):
    rows, width = glu_value.shape
    klen = conv_taps.shape[0]
    out_cols = out_grad.shape[1]
    n_sp, n_tp = lax.axis_size("sp"), lax.axis_size("tp")
    halo = -(-(klen - 1) // 16) * 16
    own = width // n_sp
    fused = width % n_sp == 0 and own % 16 == 0
    halves = width // LANES
    blocks = rows // BLOCK
    peers = max(n_sp - 1, 1) if fused else 1
    cfg = (rows, width, klen, halo, n_sp, n_tp, fused)
    rs_shape = (n_sp, own, out_cols) if fused else (1, 16, out_cols)
    vm, dma = pltpu.VMEM, pltpu.SemaphoreType.DMA
    slots = max(n_tp - 1, 1)
    scratch = [
        vm((rows, width), BF16), vm((rows, width), BF16),
        vm((width, out_cols), BF16), vm((rows, out_cols), BF16),
        vm((halo, width), BF16), vm((halo, width), BF16),
        vm((halves, rows, LANES), F32),
        vm((halves, rows + halo, LANES), F32),
        vm((halves, rows, LANES), F32),
        vm((halves, rows + halo, LANES), F32),
        vm((width, rows), BF16),
        vm((klen, 8, width), F32), vm((klen + 1, 8, width), F32),
        vm((16, LANES), F32), vm((slots, 16, LANES), F32),
        vm((16, LANES), F32), vm((slots, 16, LANES), F32),
        vm(rs_shape, BF16), vm(rs_shape, F32), vm((peers,) + rs_shape[1:], BF16),
        vm((klen + 1, width), BF16), vm((peers, klen + 1, width), BF16),
        vm((rows, width), BF16), vm((rows, width), BF16),
        dma((4,)), dma((2, blocks)), dma((2,)), dma((2,)), dma, dma,
        dma((slots,)), dma((slots,)), dma((slots,)), dma((slots,)),
        dma((peers,)), dma((peers,)), dma((peers,)), dma((peers,)),
    ]
    anywhere = pl.BlockSpec(memory_space=pl.ANY)
    vmem = pl.BlockSpec(memory_space=pltpu.VMEM)
    proj_rows = own if fused else width
    value_grad, gate_grad, proj, taps = pl.pallas_call(
        functools.partial(kernel, cfg),
        out_shape=(
            jax.ShapeDtypeStruct((rows, width), BF16),
            jax.ShapeDtypeStruct((rows, width), BF16),
            jax.ShapeDtypeStruct((proj_rows, out_cols), F32),
            jax.ShapeDtypeStruct((klen + 1, width), F32),
        ),
        in_specs=[anywhere, anywhere, vmem, vmem, anywhere, anywhere],
        out_specs=(anywhere, anywhere, vmem, vmem),
        scratch_shapes=scratch,
        compiler_params=pltpu.CompilerParams(
            collective_id=0, has_side_effects=True, vmem_limit_bytes=60 * 1024 * 1024
        ),
    )(glu_value, glu_gate, conv_taps, channel_gain[None, :], proj_weight, out_grad)
    if not fused:
        proj = lax.psum_scatter(proj, "sp", scatter_dimension=0, tiled=True)
        taps = lax.psum(taps, "sp")
    return value_grad, gate_grad, proj, taps[:klen], taps[klen]


def solution(mesh):
    from jax.sharding import PartitionSpec as P

    return jax.shard_map(
        per_device,
        mesh=mesh,
        in_specs=(
            P("sp", "tp"),
            P("sp", "tp"),
            P(None, "tp"),
            P("tp"),
            P("tp", None),
            P("sp", None),
        ),
        out_specs=(P("sp", "tp"), P("sp", "tp"), P(("tp", "sp"), None), P(None, "tp"), P("tp")),
        check_vma=False,
    )
```

time: 127 us -> 41.8 us (0.33)
  blocking collectives: 60.2 us -> 0 us
  Pallas kernels: 0 us -> 34.5 us
  other arithmetic: 20.9 us -> 0 us
  starting transfers between devices: 14.9 us -> 0 us
  between operations: 14.3 us -> 0.66 us
  matrix products: 4.72 us -> 0 us
  local copies, waits for them, and re-layouts: 10.4 us -> 6.34 us
    psum x3 -> x0, blocking collectives: 60.2 us -> none  [the longest x1 39.9 us: per_device(): taps_grad, norm_gain_gradient = lax.psum((taps_term, gain_product), 'sp')]
    pallas_call x0 -> x1, Pallas kernels: none -> 34.5 us  [per_device(): pl.pallas_call(functools.partial(kernel, cfg), out_shape=(jax.ShapeDtypeS...]
    ppermute x5 -> x0, starting transfers between devices: 14.8 us -> none  [from_behind(): return lax.ppermute(block, axis, route)]
    reduce_sum x5 -> x0, other arithmetic: 9.65 us -> none  [the longest x1 5.4 us: per_device(): jnp.sum(convolved_output * convolved_output, axis=1)]
    convert_element_type x2 -> x0, other arithmetic: 7.13 us -> none  [the longest x1 6.04 us: per_device(): (glu_grad * value_f * gate_sig * (1.0 - gate_sig)).astype(jnp.bfloat16)]
    dot_general x2 -> x0, matrix products: 4.72 us -> none  [the longest x1 2.98 us: per_device(): lax.dot_general(cot_ext, proj_weight, (((1,), (1,)), ((), ())), preferred...]
    concatenate x2 -> x0, local copies, waits for them, and re-layouts: 4.07 us -> none  [the longest x1 3.1 us: per_device(): gate_ext = jnp.concatenate([prev_gate, glu_gate, next_gate], axis=0)]
    unnamed x16 -> x8, local copies, waits for them, and re-layouts: 1.78 us -> 5.01 us
  transfers between devices with their start and end apart: 6 -> 0, of which waited for: 1 -> 0; matrix products, arithmetic and copies ran while one was open for 26% -> 0% of each run, Pallas kernels for 0% -> 0%
where the time goes in v1:
time: 41.8 us; the launch traced here: 41.5 us
  Pallas kernels  34.5 us (83%)
  local copies, waits for them, and re-layouts  6.34 us (15%)
  between operations  0.66 us (2%)
    pallas_call x1, Pallas kernels, per_device(): pl.pallas_call(functools.partial(kernel, cfg), out_shape=(jax.ShapeDtypeS...  34.5 us
    unnamed x8, local copies, waits for them, and re-layouts  5.01 us
    slice x1, local copies, waits for them, and re-layouts, per_device(): return (value_grad, gate_grad, proj, taps[:klen], taps[klen])  1.32 us

profile of v1, /device:TPU:0, one launch (start us, length us, event | category | flops | bytes accessed | tf_op | source)
XLA Modules:
  0.0 41.5 jit_solution(16140366973665660838)
XLA Ops:
  0.6 34.5 %shard_map.101 = (bf16[1024,256]{1,0:T(8,128)(2,1)}, bf16[1024,256]{1,0:T(8,128)(2,1)}, f32[32,1024]{1,0:T(8,128)}, f32[32,256]{1,0:T(8,128)}) custom-call(bf16[1024,256]{1,0:T(8,128)(2,1)} %value_hbm.1, bf16[1024,256]{1,0:T(8,128)(2,1)} %gate_hbm.1, f32[31,256]{1,0:T(8,128)} %taps_ref.1, f32[1,256]{1,0:T(1,128)} %bitcast.5, bf16[256,1024]{1,0:T(8,128)(2,1)} %weight_hbm.1, ...), custom_call_target="tpu_custom_call" | custom-call | tf_op jit(solution)/shard_map/pallas_call | solution.py:450
  35.1 0.0 copy-start
  35.1 0.0 copy-start.1
  35.2 1.3 %slice.7 = f32[1,256]{1,0:T(1,128)} slice(f32[32,256]{1,0:T(8,128)} %get-tuple-element.12), slice={[31:32], [0:256]} | slice | bytes 2048 | tf_op jit(solution)/shard_map/slice | solution.py:468
  36.5 1.9 %copy.15 = bf16[1024,256]{1,0:T(8,128)(2,1)} copy(bf16[1024,256]{1,0:T(8,128)(2,1)} %get-tuple-element.18) | data formatting | bytes 1048576
  38.4 1.9 %copy.16 = bf16[1024,256]{1,0:T(8,128)(2,1)} copy(bf16[1024,256]{1,0:T(8,128)(2,1)} %get-tuple-element.19) | data formatting | bytes 1048576
  40.2 0.0 copy-done
  40.2 0.7 %copy.17 = f32[32,1024]{1,0:T(8,128)} copy(f32[32,1024]{1,0:T(8,128)S(1)} %copy-done) | data formatting | bytes 262144
  40.9 0.0 copy-done.1
  40.9 0.6 %copy.18 = f32[31,256]{1,0:T(8,128)} copy(f32[31,256]{1,0:T(8,128)S(1)} %bitcast.3) | data formatting | bytes 63488
Async XLA Ops:
  35.1 5.1 %copy-start = (f32[32,1024]{1,0:T(8,128)S(1)}, f32[32,1024]{1,0:T(8,128)}, u32[]{:S(2)}) copy-start(f32[32,1024]{1,0:T(8,128)} %get-tuple-element.20) | copy-start | bytes 393220
  35.1 5.7 %copy-start.1 = (f32[32,256]{1,0:T(8,128)S(1)}, f32[32,256]{1,0:T(8,128)}, u32[]{:S(2)}) copy-start(f32[32,256]{1,0:T(8,128)} %get-tuple-element.12) | copy-start | bytes 98308

commit v2 on v1

--- a/solution.py
+++ b/solution.py
@@ -37,11 +37,11 @@
 def kernel(
     cfg,
     value_hbm, gate_hbm, taps_ref, gain_ref, weight_hbm, cot_hbm,
-    vgrad_hbm, ggrad_hbm, proj_out, taps_out,
-    value_v, gate_v, weight_v, cot_v, halo_v, halo_g, gsig, glu, xbuf, cg, act_t,
+    vout, gout, proj_out, taps_out,
+    value_v, gate_v, weight_v, cot_v, halo_v, halo_g, gsig, nsig, glu, xbuf, cg, act_t,
     taps_b, taps_acc, st1, st1_in, st2, st2_in, rs_send, rs_own, rs_in,
-    tg_send, tg_in, vout, gout,
-    in_sem, out_sem, halo_send, halo_recv, cgs_send, cgs_recv,
+    tg_send, tg_in,
+    in_sem, halo_send, halo_recv, cgs_send, cgs_recv,
     s1_send, s1_recv, s2_send, s2_recv, rs_ssem, rs_rsem, tg_ssem, tg_rsem,
 ):
     rows, width, klen, halo, n_sp, n_tp, fused = cfg
@@ -81,8 +81,6 @@
 
     loads[0].wait()
     loads[1].wait()
-    pl.semaphore_wait(barrier, len(sp_hops) + n_tp - 1)
-
     nxt = (jnp.minimum(sp + 1, n_sp - 1), tp)
     prv = (jnp.maximum(sp - 1, 0), tp)
 
@@ -96,11 +94,6 @@
             for i, (src, dst) in enumerate([(value_v, halo_v), (gate_v, halo_g)])
         ]
 
-    @pl.when(sp < n_sp - 1)
-    def _():
-        for copy in halo_copies():
-            copy.start()
-
     def rows_of(c):
         return pl.ds(pl.multiple_of(c * BLOCK, BLOCK), BLOCK)
 
@@ -116,6 +109,12 @@
         return carry
 
     lax.fori_loop(0, blocks, glu_block, 0)
+    pl.semaphore_wait(barrier, len(sp_hops) + n_tp - 1)
+
+    @pl.when(sp < n_sp - 1)
+    def _():
+        for copy in halo_copies():
+            copy.start()
 
     def conv_block(src, h, base, first, tap_of):
         cols = slice(h * LANES, (h + 1) * LANES)
@@ -224,36 +223,22 @@
 
     cols1 = columns(mean, rstd)
 
-    def norm_block(c, carry):
+    def activ_block(c, carry):
         at = rows_of(c)
         mean_b, rstd_b = spread(cols1, c)
-        firsts, seconds, activs = [], [], []
+        activs = []
         for h in range(halves):
             cols = slice(h * LANES, (h + 1) * LANES)
-            gain = gain_ref[0:1, cols]
             xhat = (xbuf[h, at, :] - mean_b) * rstd_b
-            normed = xhat * gain
+            normed = xhat * gain_ref[0:1, cols]
             sig = jax.nn.sigmoid(normed)
+            xbuf[h, at, :] = xhat
+            nsig[h, at, :] = sig
             activs.append(normed * sig)
-            ngrad = cg[h, at, :] * sig * (1.0 + normed * (1.0 - sig))
-            xgrad = ngrad * gain
-            taps_acc[klen, :, cols] += jnp.sum(
-                (ngrad * xhat).reshape(BLOCK // 8, 8, LANES), axis=0
-            )
-            xbuf[h, at, :] = xhat
-            cg[h, at, :] = xgrad
-            firsts.append(xgrad)
-            seconds.append(xgrad * xhat)
-        place_sums(st2, c, jnp.concatenate(firsts, axis=1), jnp.concatenate(seconds, axis=1))
-        activ = jnp.concatenate(activs, axis=1)
-        act_t[:, at] = jnp.transpose(activ).astype(BF16)
-        return carry
-
-    lax.fori_loop(0, blocks, norm_block, 0)
-
-    ex2 = tp_copies(st2, st2_in, s2_send, s2_recv)
-    for copy in ex2:
-        copy.start()
+        act_t[:, at] = jnp.transpose(jnp.concatenate(activs, axis=1)).astype(BF16)
+        return carry
+
+    lax.fori_loop(0, blocks, activ_block, 0)
 
     out_cols = proj_out.shape[-1]
     tile = 256
@@ -280,6 +265,30 @@
         else:
             proj_out[:, cols] = part
 
+    def norm_block(c, carry):
+        at = rows_of(c)
+        firsts, seconds = [], []
+        for h in range(halves):
+            cols = slice(h * LANES, (h + 1) * LANES)
+            gain = gain_ref[0:1, cols]
+            xhat = xbuf[h, at, :]
+            sig = nsig[h, at, :]
+            ngrad = cg[h, at, :] * sig * (1.0 + xhat * gain * (1.0 - sig))
+            xgrad = ngrad * gain
+            taps_acc[klen, :, cols] += jnp.sum(
+                (ngrad * xhat).reshape(BLOCK // 8, 8, LANES), axis=0
+            )
+            cg[h, at, :] = xgrad
+            firsts.append(xgrad)
+            seconds.append(xgrad * xhat)
+        place_sums(st2, c, jnp.concatenate(firsts, axis=1), jnp.concatenate(seconds, axis=1))
+        return carry
+
+    lax.fori_loop(0, blocks, norm_block, 0)
+
+    ex2 = tp_copies(st2, st2_in, s2_send, s2_recv)
+    for copy in ex2:
+        copy.start()
     for copy in ex2:
         copy.wait_recv()
     total = st2[...]
@@ -341,13 +350,6 @@
         for o in hops:
             tg_copy(o).start()
 
-    def out_copies(c):
-        at = rows_of(c)
-        return [
-            pltpu.make_async_copy(vout.at[at], vgrad_hbm.at[at], out_sem.at[0, c]),
-            pltpu.make_async_copy(gout.at[at], ggrad_hbm.at[at], out_sem.at[1, c]),
-        ]
-
     def grad_loop(c, carry):
         at = rows_of(c)
         base = c * BLOCK
@@ -358,8 +360,6 @@
             scaled = grad * sig
             vout[at, cols] = scaled.astype(BF16)
             gout[at, cols] = (scaled * value_v[at, cols].astype(F32) * (1.0 - sig)).astype(BF16)
-        for copy in out_copies(c):
-            copy.start()
         return carry
 
     lax.fori_loop(0, blocks - 1, grad_loop, 0)
@@ -402,12 +402,19 @@
     def _():
         cg_copy.wait_send()
 
-    def drain(c, carry):
-        for copy in out_copies(c):
-            copy.wait()
-        return carry
-
-    lax.fori_loop(0, blocks, drain, 0)
+
+def finish_kernel(
+    value_ref, gate_ref, proj_ref, taps_ref, value_out, gate_out, proj_out, taps_out, gain_out, sem
+):
+    pairs = [(value_ref, value_out), (gate_ref, gate_out), (proj_ref, proj_out)]
+    copies = [pltpu.make_async_copy(a, b, sem.at[i]) for i, (a, b) in enumerate(pairs)]
+    for copy in copies:
+        copy.start()
+    klen = taps_out.shape[0]
+    taps_out[...] = taps_ref[0:klen, :]
+    gain_out[...] = taps_ref[klen : klen + 1, :]
+    for copy in copies:
+        copy.wait()
 
 
 def per_device(glu_value, glu_gate, conv_taps, channel_gain, proj_weight, out_grad):
@@ -429,7 +436,7 @@
         vm((rows, width), BF16), vm((rows, width), BF16),
         vm((width, out_cols), BF16), vm((rows, out_cols), BF16),
         vm((halo, width), BF16), vm((halo, width), BF16),
-        vm((halves, rows, LANES), F32),
+        vm((halves, rows, LANES), F32), vm((halves, rows, LANES), F32),
         vm((halves, rows + halo, LANES), F32),
         vm((halves, rows, LANES), F32),
         vm((halves, rows + halo, LANES), F32),
@@ -439,33 +446,47 @@
         vm((16, LANES), F32), vm((slots, 16, LANES), F32),
         vm(rs_shape, BF16), vm(rs_shape, F32), vm((peers,) + rs_shape[1:], BF16),
         vm((klen + 1, width), BF16), vm((peers, klen + 1, width), BF16),
-        vm((rows, width), BF16), vm((rows, width), BF16),
-        dma((4,)), dma((2, blocks)), dma((2,)), dma((2,)), dma, dma,
+        dma((4,)), dma((2,)), dma((2,)), dma, dma,
         dma((slots,)), dma((slots,)), dma((slots,)), dma((slots,)),
         dma((peers,)), dma((peers,)), dma((peers,)), dma((peers,)),
     ]
-    anywhere = pl.BlockSpec(memory_space=pl.ANY)
+    hbm = pl.BlockSpec(memory_space=pltpu.HBM)
     vmem = pl.BlockSpec(memory_space=pltpu.VMEM)
     proj_rows = own if fused else width
+    out_bytes = 4 * (rows * width + proj_rows * out_cols + (klen + 1) * width)
     value_grad, gate_grad, proj, taps = pl.pallas_call(
         functools.partial(kernel, cfg),
         out_shape=(
-            jax.ShapeDtypeStruct((rows, width), BF16),
-            jax.ShapeDtypeStruct((rows, width), BF16),
-            jax.ShapeDtypeStruct((proj_rows, out_cols), F32),
-            jax.ShapeDtypeStruct((klen + 1, width), F32),
+            pltpu.VMEM((rows, width), BF16),
+            pltpu.VMEM((rows, width), BF16),
+            pltpu.VMEM((proj_rows, out_cols), F32),
+            pltpu.VMEM((klen + 1, width), F32),
         ),
-        in_specs=[anywhere, anywhere, vmem, vmem, anywhere, anywhere],
-        out_specs=(anywhere, anywhere, vmem, vmem),
+        in_specs=[hbm, hbm, vmem, vmem, hbm, hbm],
+        out_specs=(vmem, vmem, vmem, vmem),
         scratch_shapes=scratch,
         compiler_params=pltpu.CompilerParams(
-            collective_id=0, has_side_effects=True, vmem_limit_bytes=60 * 1024 * 1024
+            collective_id=0, has_side_effects=True, vmem_limit_bytes=65 * 1024 * 1000 - out_bytes
         ),
     )(glu_value, glu_gate, conv_taps, channel_gain[None, :], proj_weight, out_grad)
     if not fused:
         proj = lax.psum_scatter(proj, "sp", scatter_dimension=0, tiled=True)
         taps = lax.psum(taps, "sp")
-    return value_grad, gate_grad, proj, taps[:klen], taps[klen]
+    value_grad, gate_grad, proj, taps_grad, gain_grad = pl.pallas_call(
+        finish_kernel,
+        out_shape=(
+            jax.ShapeDtypeStruct((rows, width), BF16),
+            jax.ShapeDtypeStruct((rows, width), BF16),
+            jax.ShapeDtypeStruct(proj.shape, F32),
+            jax.ShapeDtypeStruct((klen, width), F32),
+            jax.ShapeDtypeStruct((1, width), F32),
+        ),
+        in_specs=[vmem] * 4,
+        out_specs=(hbm, hbm, hbm, vmem, vmem),
+        scratch_shapes=[dma((3,))],
+        compiler_params=pltpu.CompilerParams(vmem_limit_bytes=8 * 1024 * 1024),
+    )(value_grad, gate_grad, proj, taps)
+    return value_grad, gate_grad, proj, taps_grad, gain_grad[0]
 
 
 def solution(mesh):

time: 41.8 us -> 34.9 us (0.83)
  local copies, waits for them, and re-layouts: 6.34 us -> 0 us
  Pallas kernels: 34.5 us -> 34 us
    unnamed x8 -> x0, local copies, waits for them, and re-layouts: 5.01 us -> none
    slice x1 -> x0, local copies, waits for them, and re-layouts: 1.32 us -> none  [per_device(): return (value_grad, gate_grad, proj, taps[:klen], taps[klen])]
    pallas_call x1 -> x2, Pallas kernels: 34.5 us -> 34 us  [the longest x1 32.4 us: per_device(): pl.pallas_call(functools.partial(kernel, cfg), out_shape=(pltpu.VMEM((row...]
where the time goes in v2:
time: 34.9 us; the launch traced here: 34.7 us
  Pallas kernels  34 us (97%)
  between operations  0.64 us (2%)
    pallas_call x1, Pallas kernels, per_device(): pl.pallas_call(functools.partial(kernel, cfg), out_shape=(pltpu.VMEM((row...  32.4 us
    pallas_call x1, Pallas kernels, per_device(): pl.pallas_call(finish_kernel, out_shape=(jax.ShapeDtypeStruct((rows, widt...  1.65 us

profile of v2, /device:TPU:0, one launch (start us, length us, event | category | flops | bytes accessed | tf_op | source)
XLA Modules:
  0.0 34.7 jit_solution(5213986891988587791)
XLA Ops:
  0.6 32.4 %shard_map.101 = (bf16[1024,256]{1,0:T(8,128)(2,1)S(1)}, bf16[1024,256]{1,0:T(8,128)(2,1)S(1)}, f32[32,1024]{1,0:T(8,128)S(1)}, f32[32,256]{1,0:T(8,128)S(1)}) custom-call(bf16[1024,256]{1,0:T(8,128)(2,1)} %value_hbm.1, bf16[1024,256]{1,0:T(8,128)(2,1)} %gate_hbm.1, f32[31,256]{1,0:T(8,128)} %taps_ref.1, f32[1,256]{1,0:T(1,128)} %bitcast.2, ...), custom_call_target="tpu_custom_call" | custom-call | tf_op jit(solution)/shard_map/pallas_call | solution.py:457
  33.0 1.6 %shard_map.102 = (bf16[1024,256]{1,0:T(8,128)(2,1)}, bf16[1024,256]{1,0:T(8,128)(2,1)}, f32[32,1024]{1,0:T(8,128)}, f32[31,256]{1,0:T(8,128)}, f32[1,256]{1,0:T(1,128)}) custom-call(bf16[1024,256]{1,0:T(8,128)(2,1)S(1)} %get-tuple-element.14.value_ref, bf16[1024,256]{1,0:T(8,128)(2,1)S(1)} %get-tuple-element.15.gate_ref, ...), custom_call_target="tpu_custom_call" | custom-call | tf_op jit(solution)/shard_map/pallas_call | solution.py:475

commit v3 on v2

--- a/solution.py
+++ b/solution.py
@@ -36,9 +36,9 @@
 
 def kernel(
     cfg,
-    value_hbm, gate_hbm, taps_ref, gain_ref, weight_hbm, cot_hbm,
+    value_hbm, gate_hbm, taps_hbm, gain_hbm, weight_hbm, cot_hbm,
     vout, gout, proj_out, taps_out,
-    value_v, gate_v, weight_v, cot_v, halo_v, halo_g, gsig, nsig, glu, xbuf, cg, act_t,
+    taps_ref, gain_ref, value_v, gate_v, weight_v, cot_v, halo_v, halo_g, gsig, nsig, glu, xbuf, cg, act_t,
     taps_b, taps_acc, st1, st1_in, st2, st2_in, rs_send, rs_own, rs_in,
     tg_send, tg_in,
     in_sem, halo_send, halo_recv, cgs_send, cgs_recv,
@@ -56,12 +56,14 @@
     loads = [
         pltpu.make_async_copy(src, dst, in_sem.at[i])
         for i, (src, dst) in enumerate(
-            [(value_hbm, value_v), (gate_hbm, gate_v), (weight_hbm, weight_v), (cot_hbm, cot_v)]
+            [
+                (value_hbm, value_v), (gate_hbm, gate_v), (weight_hbm, weight_v),
+                (cot_hbm, cot_v), (taps_hbm, taps_ref), (gain_hbm, gain_ref),
+            ]
         )
     ]
-    for copy in loads:
-        copy.start()
-
+    for i in (0, 1, 4, 5, 2, 3):
+        loads[i].start()
     barrier = pltpu.get_barrier_semaphore()
     sp_hops = list(range(1, n_sp)) if fused else [1, n_sp - 1]
     for o in sp_hops:
@@ -73,8 +75,6 @@
             barrier, inc=1, device_id=(sp, lax.rem(tp + o, n_tp)), device_id_type=MESH
         )
 
-    for k in range(klen):
-        taps_b[k] = jnp.broadcast_to(taps_ref[k : k + 1, :], (8, width))
     taps_acc[...] = jnp.zeros_like(taps_acc)
     st1[...] = jnp.zeros_like(st1)
     st2[...] = jnp.zeros_like(st2)
@@ -109,6 +109,10 @@
         return carry
 
     lax.fori_loop(0, blocks, glu_block, 0)
+    loads[4].wait()
+    loads[5].wait()
+    for k in range(klen):
+        taps_b[k] = jnp.broadcast_to(taps_ref[k : k + 1, :], (8, width))
     pl.semaphore_wait(barrier, len(sp_hops) + n_tp - 1)
 
     @pl.when(sp < n_sp - 1)
@@ -154,26 +158,24 @@
         x = jnp.concatenate(parts, axis=1)
         place_sums(st1, c, x, x * x)
 
-    def fwd_loop(c, carry):
-        forward_block(c)
-        return carry
-
-    lax.fori_loop(1, blocks, fwd_loop, 0)
-
-    @pl.when(sp > 0)
-    def _():
-        for copy in halo_copies():
-            copy.wait_recv()
-        out = halo_v[...].astype(F32) * jax.nn.sigmoid(halo_g[...].astype(F32))
-        for h in range(halves):
-            glu[h, 0:halo, :] = out[:, h * LANES : (h + 1) * LANES]
-
-    @pl.when(sp == 0)
-    def _():
-        for h in range(halves):
-            glu[h, 0:halo, :] = jnp.zeros((halo, LANES), F32)
-
-    lax.fori_loop(0, 1, fwd_loop, 0)
+    def fwd_loop(i, carry):
+        @pl.when((i == blocks - 1) & (sp > 0))
+        def _():
+            for copy in halo_copies():
+                copy.wait_recv()
+            out = halo_v[...].astype(F32) * jax.nn.sigmoid(halo_g[...].astype(F32))
+            for h in range(halves):
+                glu[h, 0:halo, :] = out[:, h * LANES : (h + 1) * LANES]
+
+        @pl.when((i == blocks - 1) & (sp == 0))
+        def _():
+            for h in range(halves):
+                glu[h, 0:halo, :] = jnp.zeros((halo, LANES), F32)
+
+        forward_block(lax.rem(i + 1, blocks))
+        return carry
+
+    lax.fori_loop(0, blocks, fwd_loop, 0)
 
     def tp_copies(src, dst, ssem, rsem):
         return [
@@ -320,20 +322,19 @@
 
     def cgrad_loop(c, carry):
         cgrad_block(c)
-        return carry
-
-    lax.fori_loop(0, 1, cgrad_loop, 0)
+
+        @pl.when((c == 0) & (sp > 0))
+        def _():
+            cg_copy.start()
+
+        return carry
 
     cg_copy = pltpu.make_async_remote_copy(
         src_ref=cg.at[:, pl.ds(0, halo), :], dst_ref=cg.at[:, pl.ds(rows, halo), :],
         send_sem=cgs_send, recv_sem=cgs_recv, device_id=prv, device_id_type=MESH,
     )
 
-    @pl.when(sp > 0)
-    def _():
-        cg_copy.start()
-
-    lax.fori_loop(1, blocks, cgrad_loop, 0)
+    lax.fori_loop(0, blocks, cgrad_loop, 0)
 
     taps_sum = jnp.sum(taps_acc[...], axis=1) * factor
     taps_out[...] = taps_sum
@@ -351,6 +352,15 @@
             tg_copy(o).start()
 
     def grad_loop(c, carry):
+        @pl.when((c == blocks - 1) & (sp < n_sp - 1))
+        def _():
+            cg_copy.wait_recv()
+
+        @pl.when((c == blocks - 1) & (sp == n_sp - 1))
+        def _():
+            for h in range(halves):
+                cg[h, pl.ds(rows, halo), :] = jnp.zeros((halo, LANES), F32)
+
         at = rows_of(c)
         base = c * BLOCK
         for h in range(halves):
@@ -362,18 +372,7 @@
             gout[at, cols] = (scaled * value_v[at, cols].astype(F32) * (1.0 - sig)).astype(BF16)
         return carry
 
-    lax.fori_loop(0, blocks - 1, grad_loop, 0)
-
-    @pl.when(sp < n_sp - 1)
-    def _():
-        cg_copy.wait_recv()
-
-    @pl.when(sp == n_sp - 1)
-    def _():
-        for h in range(halves):
-            cg[h, pl.ds(rows, halo), :] = jnp.zeros((halo, LANES), F32)
-
-    lax.fori_loop(blocks - 1, blocks, grad_loop, 0)
+    lax.fori_loop(0, blocks, grad_loop, 0)
 
     if fused:
         taps_total = taps_sum
@@ -433,6 +432,7 @@
     vm, dma = pltpu.VMEM, pltpu.SemaphoreType.DMA
     slots = max(n_tp - 1, 1)
     scratch = [
+        vm((klen, width), F32), vm((1, width), F32),
         vm((rows, width), BF16), vm((rows, width), BF16),
         vm((width, out_cols), BF16), vm((rows, out_cols), BF16),
         vm((halo, width), BF16), vm((halo, width), BF16),
@@ -446,7 +446,7 @@
         vm((16, LANES), F32), vm((slots, 16, LANES), F32),
         vm(rs_shape, BF16), vm(rs_shape, F32), vm((peers,) + rs_shape[1:], BF16),
         vm((klen + 1, width), BF16), vm((peers, klen + 1, width), BF16),
-        dma((4,)), dma((2,)), dma((2,)), dma, dma,
+        dma((6,)), dma((2,)), dma((2,)), dma, dma,
         dma((slots,)), dma((slots,)), dma((slots,)), dma((slots,)),
         dma((peers,)), dma((peers,)), dma((peers,)), dma((peers,)),
     ]
@@ -462,7 +462,7 @@
             pltpu.VMEM((proj_rows, out_cols), F32),
             pltpu.VMEM((klen + 1, width), F32),
         ),
-        in_specs=[hbm, hbm, vmem, vmem, hbm, hbm],
+        in_specs=[hbm] * 6,
         out_specs=(vmem, vmem, vmem, vmem),
         scratch_shapes=scratch,
         compiler_params=pltpu.CompilerParams(

time: 34.9 us -> 34.2 us (0.980)
  Pallas kernels: 34 us -> 33.4 us
    pallas_call x1, Pallas kernels: 32.4 us -> 31.8 us  [per_device(): pl.pallas_call(functools.partial(kernel, cfg), out_shape=(pltpu.VMEM((row...]
where the time goes in v3:
time: 34.2 us; the launch traced here: 34.1 us
  Pallas kernels  33.4 us (98%)
  between operations  0.64 us (2%)
    pallas_call x1, Pallas kernels, per_device(): pl.pallas_call(functools.partial(kernel, cfg), out_shape=(pltpu.VMEM((row...  31.8 us
    pallas_call x1, Pallas kernels, per_device(): pl.pallas_call(finish_kernel, out_shape=(jax.ShapeDtypeStruct((rows, widt...  1.65 us

profile of v3, /device:TPU:0, one launch (start us, length us, event | category | flops | bytes accessed | tf_op | source)
XLA Modules:
  0.0 34.1 jit_solution(18222121977661413870)
XLA Ops:
  0.6 31.8 %shard_map.101 = (bf16[1024,256]{1,0:T(8,128)(2,1)S(1)}, bf16[1024,256]{1,0:T(8,128)(2,1)S(1)}, f32[32,1024]{1,0:T(8,128)S(1)}, f32[32,256]{1,0:T(8,128)S(1)}) custom-call(bf16[1024,256]{1,0:T(8,128)(2,1)} %value_hbm.1, bf16[1024,256]{1,0:T(8,128)(2,1)} %gate_hbm.1, f32[31,256]{1,0:T(8,128)} %taps_hbm.1, f32[1,256]{1,0:T(1,128)} %bitcast.2, ...), custom_call_target="tpu_custom_call" | custom-call | tf_op jit(solution)/shard_map/pallas_call | solution.py:457
  32.4 1.6 %shard_map.102 = (bf16[1024,256]{1,0:T(8,128)(2,1)}, bf16[1024,256]{1,0:T(8,128)(2,1)}, f32[32,1024]{1,0:T(8,128)}, f32[31,256]{1,0:T(8,128)}, f32[1,256]{1,0:T(1,128)}) custom-call(bf16[1024,256]{1,0:T(8,128)(2,1)S(1)} %get-tuple-element.14.value_ref, bf16[1024,256]{1,0:T(8,128)(2,1)S(1)} %get-tuple-element.15.gate_ref, ...), custom_call_target="tpu_custom_call" | custom-call | tf_op jit(solution)/shard_map/pallas_call | solution.py:475
